TPU v7x, 32 devices: a whole 2x2x4 slice. The times are simulated.
32 devices in a mesh: sp: 16 (over z, y, core), tp: 2 (over x).
Axes of the slice: x: 2, y: 2, z: 4, core: 2. Of those that a mesh axis runs over, the one named last changes fastest.
Arguments:
- query_rows: bfloat16 [8192, 1024], P(('sp', 'tp')), may hold values from -6 to 6
- key_rows: bfloat16 [8192, 1024], P(('sp', 'tp')), may hold values from -6 to 6
- value_rows: bfloat16 [8192, 1024], P(('sp', 'tp')), may hold values from -6 to 6
- out_grad: bfloat16 [8192, 1024], P(('sp', 'tp')), may hold values from -40 to 40
- log_totals: float32 [8192, 8], P(('sp', 'tp')), may hold values from 6 to 7.5
- out_dot: float32 [8192, 8], P(('sp', 'tp')), may hold values from -6 to 6
- bias_table: float32 [8, 320], replicated, may hold values from -4 to 4
Outputs:
- grad_query: bfloat16 [8192, 1024], P(('sp', 'tp'))
- grad_key: bfloat16 [8192, 1024], P(('sp', 'tp'))
- grad_value: bfloat16 [8192, 1024], P(('sp', 'tp'))
- grad_table: float32 [8, 320], replicated
All inputs are finite; a program needn't handle non-finite values.
Results may differ from a plain program's by a relative error of at most 0.005.
Values may be sent and summed in bfloat16 or wider, within the bound.
No kernel may reach another device: no remote copies, remote signals or barrier semaphores. Data moves between devices by JAX's collectives and lax.ppermute only.
A program may use at most 128 MiB of HBM per device.

v0:
```python
import jax
import jax.numpy as jnp
from jax import lax
from jax.sharding import PartitionSpec as P

SEG_LEN = 64
LEFT_SEGS = 8
REL_CLIP = 256


def passed_along(block, axis, distance):
    devices = range(lax.axis_size(axis))
    route = [(i - distance, i) for i in devices if i - distance in devices]
    return lax.ppermute(block, axis, route)


def band_matrix(diagonal_vals, row_count, col_count):
    head_count = diagonal_vals.shape[0]
    span_width = row_count + col_count - 1
    repeated = jnp.broadcast_to(diagonal_vals[:, None, :], (head_count, row_count, span_width))
    flat_rows = jnp.pad(
        repeated.reshape(head_count, row_count * span_width), ((0, 0), (0, row_count))
    )
    shaped = flat_rows.reshape(head_count, row_count, span_width + 1)[:, :, :col_count]
    return shaped[:, :, ::-1]


def diagonal_sums(matrix_vals):
    head_count, row_count, col_count = matrix_vals.shape
    span_width = row_count + col_count - 1
    flipped = jnp.pad(matrix_vals[:, :, ::-1], ((0, 0), (0, 0), (0, row_count)))
    skewed = flipped.reshape(head_count, row_count * (col_count + row_count))[
        :, : row_count * span_width
    ]
    return jnp.sum(skewed.reshape(head_count, row_count, span_width), axis=1)


def table_onehot(offset, row_count, col_count, table_len):
    diagonals = jnp.arange(row_count + col_count - 1, dtype=jnp.int32)
    distance = jnp.clip(offset + diagonals - (col_count - 1), 1 - SEG_LEN, REL_CLIP) + SEG_LEN - 1
    return (distance[:, None] == jnp.arange(table_len, dtype=jnp.int32)[None, :]).astype(
        jnp.float32
    )


def bias_block(bias_table, offset, row_count, col_count):
    onehot_map = table_onehot(offset, row_count, col_count, bias_table.shape[1])
    diagonal_vals = jnp.dot(bias_table, onehot_map.T, precision=lax.Precision.HIGHEST)
    return (band_matrix(diagonal_vals, row_count, col_count), onehot_map)


def band_stack(rows, block_count, span_segs):
    segmented = rows.reshape(-1, SEG_LEN, rows.shape[1])
    pieces = [segmented[start : start + block_count] for start in range(span_segs)]
    return jnp.stack(pieces, axis=1).reshape(block_count, span_segs * SEG_LEN, rows.shape[1])


def band_terms(queries, grads_out, log_rows, dot_rows, keys, values, bias_vals, allowed):
    block_count, query_count, feature_count = queries.shape
    key_count = keys.shape[1]
    head_count = log_rows.shape[2]
    query_heads = queries.reshape(block_count, query_count, head_count, -1)
    grad_heads = grads_out.reshape(block_count, query_count, head_count, -1)
    key_heads = keys.reshape(block_count, key_count, head_count, -1)
    value_heads = values.reshape(block_count, key_count, head_count, -1)
    inv_root = query_heads.shape[3] ** (-0.5)
    raw_scores = jnp.einsum(
        "bqhd,bkhd->bhqk", query_heads, key_heads, preferred_element_type=jnp.float32
    )
    scores = raw_scores * inv_root + bias_vals[None]
    log_terms = jnp.transpose(log_rows, (0, 2, 1))[:, :, :, None]
    dot_terms = jnp.transpose(dot_rows, (0, 2, 1))[:, :, :, None]
    weights = jnp.exp(scores - log_terms)
    weights = jnp.where(allowed[:, None, None, :], weights, 0.0)
    weight_grads = jnp.einsum(
        "bqhd,bkhd->bhqk", grad_heads, value_heads, preferred_element_type=jnp.float32
    )
    score_grads = weights * (weight_grads - dot_terms)
    return (
        weights.astype(jnp.bfloat16),
        score_grads.astype(jnp.bfloat16),
        score_grads,
        query_heads,
        key_heads,
        grad_heads,
        inv_root,
    )


def local(query_rows, key_rows, value_rows, out_grad, log_totals, out_dot, bias_table):
    row_count = query_rows.shape[0]
    feature_count = query_rows.shape[1]
    head_count = log_totals.shape[1]
    seg_count = row_count // SEG_LEN
    span_segs = LEFT_SEGS + 1
    band_len = span_segs * SEG_LEN
    need_rows = LEFT_SEGS * SEG_LEN
    lag_total = -(-need_rows // row_count)
    skip_rows = lag_total * row_count - need_rows
    first_row = lax.axis_index(("sp", "tp")) * row_count
    earlier = []
    for lag_count in range(lag_total, 0, -1):
        start_row = skip_rows if lag_count == lag_total else 0
        earlier.append(passed_along((key_rows, value_rows), ("sp", "tp"), lag_count))
    all_keys = jnp.concatenate([pair[0] for pair in earlier] + [key_rows], axis=0)
    all_values = jnp.concatenate([pair[1] for pair in earlier] + [value_rows], axis=0)
    key_bands = band_stack(all_keys, seg_count, span_segs)
    value_bands = band_stack(all_values, seg_count, span_segs)
    band_pos = (
        jnp.arange(seg_count, dtype=jnp.int32)[:, None] * SEG_LEN
        + jnp.arange(band_len, dtype=jnp.int32)[None, :]
    )
    allowed = first_row - need_rows + band_pos >= 0
    bias_vals, onehot_map = bias_block(bias_table, need_rows, SEG_LEN, band_len)
    weights_b, score_grads_b, score_grads, query_heads, key_heads, grad_heads, inv_root = (
        band_terms(
            query_rows.reshape(seg_count, SEG_LEN, feature_count),
            out_grad.reshape(seg_count, SEG_LEN, feature_count),
            log_totals.reshape(seg_count, SEG_LEN, head_count),
            out_dot.reshape(seg_count, SEG_LEN, head_count),
            key_bands,
            value_bands,
            bias_vals,
            allowed,
        )
    )
    tap_part = jnp.dot(
        diagonal_sums(jnp.sum(score_grads, axis=0)), onehot_map, precision=lax.Precision.HIGHEST
    )
    query_part = jnp.einsum(
        "bhqk,bkhd->bqhd", score_grads_b, key_heads, preferred_element_type=jnp.float32
    )
    grad_query = (query_part * inv_root).reshape(row_count, feature_count).astype(jnp.bfloat16)
    key_band_grad = jnp.einsum(
        "bhqk,bqhd->bkhd", score_grads_b, query_heads, preferred_element_type=jnp.float32
    )
    key_band_grad = (key_band_grad * inv_root).reshape(seg_count, span_segs, SEG_LEN, feature_count)
    value_band_grad = jnp.einsum(
        "bhqk,bqhd->bkhd", weights_b, grad_heads, preferred_element_type=jnp.float32
    )
    value_band_grad = value_band_grad.reshape(seg_count, span_segs, SEG_LEN, feature_count)
    key_all = sum(
        (
            jnp.pad(key_band_grad[:, lag], ((lag, LEFT_SEGS - lag), (0, 0), (0, 0)))
            for lag in range(span_segs)
        )
    ).reshape(-1, feature_count)
    value_all = sum(
        (
            jnp.pad(value_band_grad[:, lag], ((lag, LEFT_SEGS - lag), (0, 0), (0, 0)))
            for lag in range(span_segs)
        )
    ).reshape(-1, feature_count)
    key_total = key_all[need_rows:]
    value_total = value_all[need_rows:]
    for lag_count in range(1, lag_total + 1):
        lower_row = max(need_rows - lag_count * row_count, 0)
        upper_row = need_rows - (lag_count - 1) * row_count
        returned = passed_along(
            (key_all[lower_row:upper_row], value_all[lower_row:upper_row]), ("sp", "tp"), -lag_count
        )
        lead_rows = row_count - (upper_row - lower_row)
        key_total = key_total + returned[0]
        value_total = value_total + returned[1]
    grad_table = lax.psum(tap_part, ("sp", "tp"))
    return (
        grad_query,
        key_total.astype(jnp.bfloat16),
        value_total.astype(jnp.bfloat16),
        grad_table,
    )


def solution(mesh):
    placed = (
        P(("sp", "tp"), None),
        P(("sp", "tp"), None),
        P(("sp", "tp"), None),
        P(("sp", "tp"), None),
        P(("sp", "tp"), None),
        P(("sp", "tp"), None),
        P(),
    )
    return jax.shard_map(
        local,
        mesh=mesh,
        in_specs=placed,
        out_specs=(P(("sp", "tp"), None), P(("sp", "tp"), None), P(("sp", "tp"), None), P()),
        check_vma=False,
    )
```

profile of v0, /device:TPU:0, one launch (start us, length us, event | category | flops | bytes accessed | tf_op | source)
XLA Modules:
  0.0 198.3 jit_solution(5561602564015735739)
XLA Ops:
  0.6 5.7 %collective-permute-start.1 = (bf16[256,1024]{1,0:T(8,128)(2,1)}, bf16[256,1024]{1,0:T(8,128)(2,1)}, u32[]{:S(2)}, u32[]{:S(2)}) collective-permute-start(bf16[256,1024]{1,0:T(8,128)(2,1)} %param.8), channel_id=1, source_target_pairs={{0,1},{1,2},{2,3},{3,4},{4,5},{5,6},{6,7},{7,8},{8,9},{9,10},{10,1... | collective-permute-start | bytes 1572872 | tf_op jit(solution)/shard_map/ppermute | solution.py:14
  6.3 2.1 %collective-permute-start = (bf16[256,1024]{1,0:T(8,128)(2,1)}, bf16[256,1024]{1,0:T(8,128)(2,1)}, u32[]{:S(2)}, u32[]{:S(2)}) collective-permute-start(bf16[256,1024]{1,0:T(8,128)(2,1)} %param.8), channel_id=1, source_target_pairs={{0,2},{1,3},{2,4},{3,5},{4,6},{5,7},{6,8},{7,9},{8,10},{9,11},{10,... | collective-permute-start | bytes 1572872 | tf_op jit(solution)/shard_map/ppermute | solution.py:14
  8.4 4.1 %collective-permute-start.3 = (bf16[256,1024]{1,0:T(8,128)(2,1)}, bf16[256,1024]{1,0:T(8,128)(2,1)}, u32[]{:S(2)}, u32[]{:S(2)}) collective-permute-start(bf16[256,1024]{1,0:T(8,128)(2,1)} %param.9), channel_id=1, source_target_pairs={{0,1},{1,2},{2,3},{3,4},{4,5},{5,6},{6,7},{7,8},{8,9},{9,10},{10,1... | collective-permute-start | bytes 1572872 | tf_op jit(solution)/shard_map/ppermute | solution.py:14
  12.6 2.1 %collective-permute-start.2 = (bf16[256,1024]{1,0:T(8,128)(2,1)}, bf16[256,1024]{1,0:T(8,128)(2,1)}, u32[]{:S(2)}, u32[]{:S(2)}) collective-permute-start(bf16[256,1024]{1,0:T(8,128)(2,1)} %param.9), channel_id=1, source_target_pairs={{0,2},{1,3},{2,4},{3,5},{4,6},{5,7},{6,8},{7,9},{8,10},{9,11},{10,... | collective-permute-start | bytes 1572872 | tf_op jit(solution)/shard_map/ppermute | solution.py:14
  18.1 1.9 copy.175
  24.6 3.6 %collective-permute-done.3 = bf16[256,1024]{1,0:T(8,128)(2,1)} collective-permute-done((bf16[256,1024]{1,0:T(8,128)(2,1)}, bf16[256,1024]{1,0:T(8,128)(2,1)}, u32[]{:S(2)}, u32[]{:S(2)}) %collective-permute-start.3) | collective-permute-done | bytes 524320 | tf_op jit(solution)/shard_map/ppermute | solution.py:14
  39.1 1.7 fusion.5
  41.3 5.0 %convolution_bitcast_fusion = f32[4,576,8,128]{3,1,2,0:T(8,128)} fusion(f32[4,8,576,64]{2,3,1,0:T(8,128)S(1)} %fusion.5, f32[4,8,64]{2,1,0:T(8,128)S(1)} %get-tuple-element.49, f32[8,64,576]{2,1,0:T(8,128)S(1)} %slice.268, pred[4,576]{1,0:T(4,128)(4,1)S(1)} %add_compare_fusion, bf16[4,64,8,128]{3,2,1,0:T(8,128)(2,1)S(1)} %bitcast.221), kind=kOutput, calls=%fused_computation.13 | convolution fusion | flops 307888128 | bytes 15870208 | tf_op jit(solution)/shard_map/bhqk,bqhd->bkhd/dot_general | solution.py:138
  46.3 4.2 %fusion.52 = (f32[8,64,576]{2,1,0:T(8,128)S(1)}, bf16[4,8,64,576]{3,2,1,0:T(8,128)(2,1)}) fusion(f32[4,8,64]{2,1,0:T(8,128)S(1)} %get-tuple-element.48, bf16[4,64,8,128]{3,2,1,0:T(8,128)(2,1)S(1)} %bitcast.222, bf16[4,576,8,128]{3,2,1,0:T(8,128)(2,1)S(1)} %bitcast.220, f32[4,8,64]{2,1,0:T(8,128)S(1)} %get-tuple-element.49, f32[8,64,576]{2,1,0:T(8,128)S(1)} %slice.268, ...), kind=kOutput, calls=%fused_computation.101 | convolution fusion | flops 311132160 | bytes 14698752 | tf_op jit(solution)/shard_map/bqhd,bkhd->bhqk/dot_general | solution.py:75
  52.8 1.3 reshape.121
  54.2 12.8 %copy.146 = f32[4,576,8,128]{3,2,1,0:T(8,128)} copy(f32[4,576,8,128]{3,1,2,0:T(8,128)} %convolution_bitcast_fusion) | data formatting | bytes 18874368 | tf_op jit(solution)/shard_map/bhqk,bqhd->bkhd/transpose | solution.py:138
  67.0 11.2 %reshape.119 = f32[4,9,64,1024]{3,2,1,0:T(8,128)} reshape(f32[4,576,8,128]{3,2,1,0:T(8,128)} %copy.146) | data formatting | bytes 18874368 | tf_op jit(solution)/shard_map/reshape | solution.py:141
  78.2 4.7 %slice_bitcast_fusion.8 = (f32[4,64,1024]{2,1,0:T(8,128)S(1)}, f32[4,64,1024]{2,1,0:T(8,128)S(1)}, f32[4,64,1024]{2,1,0:T(8,128)S(1)}, f32[4,64,1024]{2,1,0:T(8,...) fusion(f32[4,9,64,1024]{3,2,1,0:T(8,128)} %reshape.119), kind=kLoop, calls=%fused_computation.37 | loop fusion | bytes 18874368 | tf_op jit(solution)/shard_map/squeeze | solution.py:150
  83.8 1.6 fusion.46
  86.8 1.5 collective-permute-start.6
  88.3 1.5 multiply_bitcast_fusion
  89.8 9.1 %copy.136 = f32[4,576,8,128]{3,2,1,0:T(8,128)} copy(f32[4,576,8,128]{3,1,2,0:T(8,128)S(1)} %multiply_bitcast_fusion) | data formatting | bytes 18874368 | tf_op jit(solution)/shard_map/mul | solution.py:137
  98.9 11.1 %reshape.118 = f32[4,9,64,1024]{3,2,1,0:T(8,128)} reshape(f32[4,576,8,128]{3,2,1,0:T(8,128)} %copy.136) | data formatting | bytes 18874368 | tf_op jit(solution)/shard_map/reshape | solution.py:137
  110.0 4.7 %slice_bitcast_fusion.17 = (f32[4,64,1024]{2,1,0:T(8,128)S(1)}, f32[4,64,1024]{2,1,0:T(8,128)S(1)}, f32[4,64,1024]{2,1,0:T(8,128)S(1)}, f32[4,64,1024]{2,1,0:T(8...) fusion(f32[4,9,64,1024]{3,2,1,0:T(8,128)} %reshape.118), kind=kLoop, calls=%fused_computation.46 | loop fusion | bytes 18874368 | tf_op jit(solution)/shard_map/squeeze | solution.py:144
  115.8 1.7 fusion.47
  117.5 1.4 collective-permute-start.5
  123.2 70.2 %psum.7 = f32[8,320]{1,0:T(8,128)} all-reduce(f32[8,320]{1,0:T(8,128)S(1)} %fusion.37), channel_id=1, replica_groups=mesh['sp'=16,'tp'=2] {'sp','tp'}, use_global_device_ids=true, to_apply=%region_2.3 | all-reduce | flops 2560 | bytes 20480 | tf_op jit(solution)/shard_map/psum | solution.py:165
  193.4 2.6 %fusion.34 = bf16[256,1024]{1,0:T(8,128)(2,1)} fusion(f32[256,1024]{1,0:T(8,128)} %collective-permute-done.7, f32[256,1024]{1,0:T(8,128)} %collective-permute-done.6, f32[4,64,1024]{2,1,0:T(8,128)S(1)} %get-tuple-element.22), kind=kLoop, calls=%fused_computation.49 | loop fusion | flops 786432 | bytes 3670016 | tf_op jit(solution)/shard_map/convert_element_type | solution.py:169
  196.0 2.3 %fusion.36 = bf16[256,1024]{1,0:T(8,128)(2,1)} fusion(f32[256,1024]{1,0:T(8,128)S(1)} %collective-permute-done.5, f32[256,1024]{1,0:T(8,128)} %collective-permute-done.4, f32[4,64,1024]{2,1,0:T(8,128)S(1)} %get-tuple-element.25), kind=kLoop, calls=%fused_computation.52 | loop fusion | flops 786432 | bytes 3670016 | tf_op jit(solution)/shard_map/convert_element_type | solution.py:168
  (83 shorter events, 28.8 us)
Async XLA Ops:
  0.6 14.0 %copy-start = (f32[8,320]{1,0:T(8,128)S(1)}, f32[8,320]{1,0:T(8,128)}, u32[]{:S(2)}) copy-start(f32[8,320]{1,0:T(8,128)} %param.13) | copy-start | bytes 30724
  0.6 29.3 %collective-permute-start.1 = (bf16[256,1024]{1,0:T(8,128)(2,1)}, bf16[256,1024]{1,0:T(8,128)(2,1)}, u32[]{:S(2)}, u32[]{:S(2)}) collective-permute-start(bf16[256,1024]{1,0:T(8,128)(2,1)} %param.8), channel_id=1, source_target_pairs={{0,1},{1,2},{2,3},{3,4},{4,5},{5,6},{6,7},{7,8},{8,9},{9,10},{10,1... | collective-permute-start | bytes 1572872 | tf_op jit(solution)/shard_map/ppermute | solution.py:14
  6.3 17.2 %collective-permute-start = (bf16[256,1024]{1,0:T(8,128)(2,1)}, bf16[256,1024]{1,0:T(8,128)(2,1)}, u32[]{:S(2)}, u32[]{:S(2)}) collective-permute-start(bf16[256,1024]{1,0:T(8,128)(2,1)} %param.8), channel_id=1, source_target_pairs={{0,2},{1,3},{2,4},{3,5},{4,6},{5,7},{6,8},{7,9},{8,10},{9,11},{10,... | collective-permute-start | bytes 1572872 | tf_op jit(solution)/shard_map/ppermute | solution.py:14
  8.4 19.8 %collective-permute-start.3 = (bf16[256,1024]{1,0:T(8,128)(2,1)}, bf16[256,1024]{1,0:T(8,128)(2,1)}, u32[]{:S(2)}, u32[]{:S(2)}) collective-permute-start(bf16[256,1024]{1,0:T(8,128)(2,1)} %param.9), channel_id=1, source_target_pairs={{0,1},{1,2},{2,3},{3,4},{4,5},{5,6},{6,7},{7,8},{8,9},{9,10},{10,1... | collective-permute-start | bytes 1572872 | tf_op jit(solution)/shard_map/ppermute | solution.py:14
  12.6 9.9 %collective-permute-start.2 = (bf16[256,1024]{1,0:T(8,128)(2,1)}, bf16[256,1024]{1,0:T(8,128)(2,1)}, u32[]{:S(2)}, u32[]{:S(2)}) collective-permute-start(bf16[256,1024]{1,0:T(8,128)(2,1)} %param.9), channel_id=1, source_target_pairs={{0,2},{1,3},{2,4},{3,5},{4,6},{5,7},{6,8},{7,9},{8,10},{9,11},{10,... | collective-permute-start | bytes 1572872 | tf_op jit(solution)/shard_map/ppermute | solution.py:14
  22.0 7.4 %copy-start.6 = (bf16[256,1024]{1,0:T(8,128)(2,1)S(1)}, bf16[256,1024]{1,0:T(8,128)(2,1)}, u32[]{:S(2)}) copy-start(bf16[256,1024]{1,0:T(8,128)(2,1)} %param.9) | copy-start | bytes 1572868
  29.4 1.7 copy-start.7
  39.0 2.2 %copy-start.2 = (bf16[288,8,8,128]{3,2,1,0:T(8,128)(2,1)}, bf16[288,8,8,128]{3,2,1,0:T(8,128)(2,1)S(1)}, u32[]{:S(2)}) copy-start(bf16[288,8,8,128]{3,2,1,0:T(8,128)(2,1)S(1)} %copy.171) | copy-start | bytes 14155780
  39.1 2.2 %copy-start.5 = (bf16[32,8,8,128]{3,2,1,0:T(8,128)(2,1)S(1)}, bf16[32,8,8,128]{3,2,1,0:T(8,128)(2,1)}, u32[]{:S(2)}) copy-start(bf16[32,8,8,128]{3,2,1,0:T(8,128)(2,1)} %copy.175) | copy-start | bytes 1572868
  83.8 4.5 %copy-start.3 = (bf16[4,8,64,576]{3,2,1,0:T(8,128)(2,1)S(1)}, bf16[4,8,64,576]{3,2,1,0:T(8,128)(2,1)}, u32[]{:S(2)}) copy-start(bf16[4,8,64,576]{3,2,1,0:T(8,128)(2,1)} %get-tuple-element.45) | copy-start | bytes 7077892
  85.5 107.9 %collective-permute-start.7 = (f32[256,1024]{1,0:T(8,128)}, f32[256,1024]{1,0:T(8,128)}, u32[]{:S(2)}, u32[]{:S(2)}) collective-permute-start(f32[256,1024]{1,0:T(8,128)} %bitcast.67), channel_id=1, source_target_pairs={{2,0},{3,1},{4,2},{5,3},{6,4},{7,5},{8,6},{9,7},{10,8},{11,9},{12,... | collective-permute-start | bytes 3145736 | tf_op jit(solution)/shard_map/ppermute | solution.py:14
  86.8 106.6 %collective-permute-start.6 = (f32[256,1024]{1,0:T(8,128)}, f32[256,1024]{1,0:T(8,128)}, u32[]{:S(2)}, u32[]{:S(2)}) collective-permute-start(f32[256,1024]{1,0:T(8,128)} %bitcast.66), channel_id=1, source_target_pairs={{1,0},{2,1},{3,2},{4,3},{5,4},{6,5},{7,6},{8,7},{9,8},{10,9},{11,1... | collective-permute-start | bytes 3145736 | tf_op jit(solution)/shard_map/ppermute | solution.py:14
  110.0 10.2 %slice-start = ((s8[4718592]{0:T(1024)(128)(4,1)}), s8[524288]{0:T(1024)(128)(4,1)S(1)}, s32[]{:S(2)}) async-start(s8[4718592]{0:T(1024)(128)(4,1)} %bitcast.210), calls=%async_computation | async-start | bytes 1048576
  114.8 5.4 %slice-start.1 = ((s8[4718592]{0:T(1024)(128)(4,1)}), s8[4194304]{0:T(1024)(128)(4,1)S(1)}, s32[]{:S(2)}) async-start(s8[4718592]{0:T(1024)(128)(4,1)} %bitcast.210), calls=%async_computation.1 | async-start | bytes 8388608
  115.8 4.4 %copy-start.4 = (bf16[4,8,64,576]{3,2,1,0:T(8,128)(2,1)S(1)}, bf16[4,8,64,576]{3,2,1,0:T(8,128)(2,1)}, u32[]{:S(2)}) copy-start(bf16[4,8,64,576]{3,2,1,0:T(8,128)(2,1)} %get-tuple-element.45) | copy-start | bytes 7077892
  117.5 78.5 %collective-permute-start.5 = (f32[256,1024]{1,0:T(8,128)}, f32[256,1024]{1,0:T(8,128)S(1)}, u32[]{:S(2)}, u32[]{:S(2)}) collective-permute-start(f32[256,1024]{1,0:T(8,128)} %bitcast.54), channel_id=1, source_target_pairs={{2,0},{3,1},{4,2},{5,3},{6,4},{7,5},{8,6},{9,7},{10,8},{11,9},{12,... | collective-permute-start | bytes 3145736 | tf_op jit(solution)/shard_map/ppermute | solution.py:14
  118.9 77.1 %collective-permute-start.4 = (f32[256,1024]{1,0:T(8,128)}, f32[256,1024]{1,0:T(8,128)}, u32[]{:S(2)}, u32[]{:S(2)}) collective-permute-start(f32[256,1024]{1,0:T(8,128)} %bitcast.53), channel_id=1, source_target_pairs={{1,0},{2,1},{3,2},{4,3},{5,4},{6,5},{7,6},{8,7},{9,8},{10,9},{11,1... | collective-permute-start | bytes 3145736 | tf_op jit(solution)/shard_map/ppermute | solution.py:14
  120.2 78.0 %copy-start.1 = (f32[8,320]{1,0:T(8,128)S(1)}, f32[8,320]{1,0:T(8,128)}, u32[]{:S(2)}) copy-start(f32[8,320]{1,0:T(8,128)} %param.13) | copy-start | bytes 30724
where the time goes:
time: 200 us; the launch traced here: 198 us
  local copies, waits for them, and re-layouts  81.9 us (41%)
  blocking collectives  70.2 us (35%)
  starting transfers between devices  19.5 us (10%)
  matrix products  14.8 us (7%)
  other arithmetic  7.04 us (4%)
  waiting for transfers between devices  3.66 us (2%)
    psum x1, blocking collectives, local(): grad_table = lax.psum(tap_part, ('sp', 'tp'))  70.2 us
    unnamed x52, local copies, waits for them, and re-layouts  19.8 us
    ppermute x8, starting transfers between devices, passed_along(): return lax.ppermute(block, axis, route)  19.5 us
    transpose x1, local copies, waits for them, and re-layouts, local(): jnp.einsum('bhqk,bqhd->bkhd', weights_b, grad_heads, preferred_element_ty...  12.8 us
    reshape x1, local copies, waits for them, and re-layouts, local(): value_band_grad.reshape(seg_count, span_segs, SEG_LEN, feature_count)  11.2 us
    reshape x1, local copies, waits for them, and re-layouts, local(): (key_band_grad * inv_root).reshape(seg_count, span_segs, SEG_LEN, feature...  11.1 us
    mul x1, local copies, waits for them, and re-layouts, local(): key_band_grad * inv_root  9.13 us
    dot_general x1, matrix products, local(): jnp.einsum('bhqk,bqhd->bkhd', weights_b, grad_heads, preferred_element_ty...  5.01 us
  transfers between devices with their start and end apart: 8, of which 1 were waited for; matrix products, arithmetic and copies ran while one was open for 23% of the time, Pallas kernels for 0%

commit v1 on v0

--- a/solution.py
+++ b/solution.py
@@ -162,7 +162,7 @@
         lead_rows = row_count - (upper_row - lower_row)
         key_total = key_total + returned[0]
         value_total = value_total + returned[1]
-    grad_table = lax.psum(tap_part, ("sp", "tp"))
+    grad_table = jnp.sum(lax.all_gather(tap_part, ("sp", "tp")), axis=0)
     return (
         grad_query,
         key_total.astype(jnp.bfloat16),

time: 200 us -> 227 us (1.14)
  blocking collectives: 70.2 us -> 92.8 us
  local copies, waits for them, and re-layouts: 81.9 us -> 85.7 us
  other arithmetic: 7.04 us -> 9.33 us
    all_gather x0 -> x1, blocking collectives: none -> 92.8 us  [local(): grad_table = jnp.sum(lax.all_gather(tap_part, ('sp', 'tp')), axis=0)]
    psum x1 -> x0, blocking collectives: 70.2 us -> none  [local(): grad_table = lax.psum(tap_part, ('sp', 'tp'))]
    unnamed x52 -> x70, local copies, waits for them, and re-layouts: 19.8 us -> 24.1 us
    transpose x1, local copies, waits for them, and re-layouts: 12.8 us -> 9.3 us  [local(): jnp.einsum('bhqk,bqhd->bkhd', weights_b, grad_heads, preferred_element_ty...]
    dot_general x1, matrix products: 5.01 us -> 2.39 us  [local(): jnp.einsum('bhqk,bqhd->bkhd', weights_b, grad_heads, preferred_element_ty...]
  transfers between devices with their start and end apart: 8 -> 8, of which waited for: 1 -> 1; matrix products, arithmetic and copies ran while one was open for 23% -> 25% of each run, Pallas kernels for 0% -> 0%
where the time goes in v1:
time: 227 us; the launch traced here: 225 us
  blocking collectives  92.8 us (41%)
  local copies, waits for them, and re-layouts  85.7 us (38%)
  starting transfers between devices  19.7 us (9%)
  matrix products  13.1 us (6%)
  other arithmetic  9.33 us (4%)
  waiting for transfers between devices  3.5 us (2%)
    all_gather x1, blocking collectives, local(): grad_table = jnp.sum(lax.all_gather(tap_part, ('sp', 'tp')), axis=0)  92.8 us
    unnamed x70, local copies, waits for them, and re-layouts  24.1 us
    ppermute x8, starting transfers between devices, passed_along(): return lax.ppermute(block, axis, route)  19.7 us
    reshape x1, local copies, waits for them, and re-layouts, local(): value_band_grad.reshape(seg_count, span_segs, SEG_LEN, feature_count)  11.1 us
    reshape x1, local copies, waits for them, and re-layouts, local(): (key_band_grad * inv_root).reshape(seg_count, span_segs, SEG_LEN, feature...  11.1 us
    transpose x1, local copies, waits for them, and re-layouts, local(): jnp.einsum('bhqk,bqhd->bkhd', weights_b, grad_heads, preferred_element_ty...  9.3 us
    mul x1, local copies, waits for them, and re-layouts, local(): key_band_grad * inv_root  9.12 us
    squeeze x1, local copies, waits for them, and re-layouts, local(): value_band_grad[:, lag]  6.41 us
  transfers between devices with their start and end apart: 8, of which 1 were waited for; matrix products, arithmetic and copies ran while one was open for 25% of the time, Pallas kernels for 0%

profile of v1, /device:TPU:0, one launch (start us, length us, event | category | flops | bytes accessed | tf_op | source)
XLA Modules:
  0.0 225.3 jit_solution(12074274174946755025)
XLA Ops:
  0.6 5.7 %collective-permute-start.1 = (bf16[256,1024]{1,0:T(8,128)(2,1)}, bf16[256,1024]{1,0:T(8,128)(2,1)}, u32[]{:S(2)}, u32[]{:S(2)}) collective-permute-start(bf16[256,1024]{1,0:T(8,128)(2,1)} %param.8), channel_id=1, source_target_pairs={{0,1},{1,2},{2,3},{3,4},{4,5},{5,6},{6,7},{7,8},{8,9},{9,10},{10,1... | collective-permute-start | bytes 1572872 | tf_op jit(solution)/shard_map/ppermute | solution.py:14
  6.3 2.1 collective-permute-start
  8.4 4.1 %collective-permute-start.3 = (bf16[256,1024]{1,0:T(8,128)(2,1)}, bf16[256,1024]{1,0:T(8,128)(2,1)}, u32[]{:S(2)}, u32[]{:S(2)}) collective-permute-start(bf16[256,1024]{1,0:T(8,128)(2,1)} %param.9), channel_id=1, source_target_pairs={{0,1},{1,2},{2,3},{3,4},{4,5},{5,6},{6,7},{7,8},{8,9},{9,10},{10,1... | collective-permute-start | bytes 1572872 | tf_op jit(solution)/shard_map/ppermute | solution.py:14
  12.6 2.1 collective-permute-start.2
  18.1 1.9 copy.175
  24.8 3.5 %collective-permute-done.3 = bf16[256,1024]{1,0:T(8,128)(2,1)} collective-permute-done((bf16[256,1024]{1,0:T(8,128)(2,1)}, bf16[256,1024]{1,0:T(8,128)(2,1)}, u32[]{:S(2)}, u32[]{:S(2)}) %collective-permute-start.3) | collective-permute-done | bytes 524320 | tf_op jit(solution)/shard_map/ppermute | solution.py:14
  33.9 3.4 %copy.174 = bf16[288,8,8,128]{3,2,1,0:T(8,128)(2,1)} copy(bf16[288,8,8,128]{3,1,2,0:T(8,128)(2,1)S(1)} %bitcast.217) | data formatting | bytes 9437184
  41.0 1.7 fusion.5
  43.1 2.3 %copy-done.2 = f32[4,8,576,64]{2,3,1,0:T(8,128)} copy-done((f32[4,8,576,64]{2,3,1,0:T(8,128)}, f32[4,8,576,64]{2,3,1,0:T(8,128)S(1)}, u32[]{:S(2)}) %copy-start.2) | copy-done | bytes 4718616
  45.4 2.4 %convolution_bitcast_fusion = f32[4,576,8,128]{3,1,2,0:T(8,128)S(1)} fusion(f32[4,8,576,64]{2,3,1,0:T(8,128)S(1)} %fusion.5, f32[4,8,64]{2,1,0:T(8,128)S(1)} %get-tuple-element.49, f32[8,64,576]{2,1,0:T(8,128)S(1)} %slice.268, pred[4,576]{1,0:T(4,128)(4,1)S(1)} %add_compare_fusion, bf16[4,64,8,128]{3,2,1,0:T(8,128)(2,1)S(1)} %bitcast.227), kind=kOutput, calls=%fused_computation.13 | convolution fusion | flops 307888128 | bytes 15870208 | tf_op jit(solution)/shard_map/bhqk,bqhd->bkhd/dot_general | solution.py:138
  47.8 9.3 %copy.146 = f32[4,576,8,128]{3,2,1,0:T(8,128)} copy(f32[4,576,8,128]{3,1,2,0:T(8,128)S(1)} %convolution_bitcast_fusion) | data formatting | bytes 18874368 | tf_op jit(solution)/shard_map/bhqk,bqhd->bkhd/transpose | solution.py:138
  57.1 11.1 %reshape.119 = f32[4,9,64,1024]{3,2,1,0:T(8,128)} reshape(f32[4,576,8,128]{3,2,1,0:T(8,128)} %copy.146) | data formatting | bytes 18874368 | tf_op jit(solution)/shard_map/reshape | solution.py:141
  68.2 6.4 %slice_bitcast_fusion.8 = (f32[4,64,1024]{2,1,0:T(8,128)S(1)}, f32[4,64,1024]{2,1,0:T(8,128)S(1)}, f32[4,64,1024]{2,1,0:T(8,128)S(1)}, f32[4,64,1024]{2,1,0:T(8,...) fusion(f32[4,9,64,1024]{3,2,1,0:T(8,128)} %reshape.119), kind=kLoop, calls=%fused_computation.37 | loop fusion | bytes 18874368 | tf_op jit(solution)/shard_map/squeeze | solution.py:150
  74.6 2.4 %pad_add_fusion = f32[12,64,1024]{2,1,0:T(8,128)S(1)} fusion(f32[4,64,1024]{2,1,0:T(8,128)} %get-tuple-element.11, f32[4,64,1024]{2,1,0:T(8,128)} %get-tuple-element.12, f32[4,64,1024]{2,1,0:T(8,128)S(1)} %get-tuple-element.5, f32[4,64,1024]{2,1,0:T(8,128)S(1)} %get-tuple-element.6, f32[4,64,1024]{2,1,0:T(8,128)S(1)} %get-tuple-element.7, ...), kind=kLoop, calls=%fused_computation.14 | loop fusion | flops 6291456 | bytes 12582912 | tf_op jit(solution)/shard_map/add | solution.py:148
  77.0 1.8 fusion.46
  81.4 4.4 %fusion.52 = (f32[8,64,576]{2,1,0:T(8,128)}, bf16[4,8,64,576]{3,2,1,0:T(8,128)(2,1)S(1)}) fusion(f32[4,8,64]{2,1,0:T(8,128)S(1)} %get-tuple-element.48, bf16[4,64,8,128]{3,2,1,0:T(8,128)(2,1)S(1)} %bitcast.228, bf16[4,576,8,128]{3,2,1,0:T(8,128)(2,1)S(1)} %bitcast.226, f32[4,8,64]{2,1,0:T(8,128)S(1)} %get-tuple-element.49, f32[8,64,576]{2,1,0:T(8,128)S(1)} %slice.268, ...), kind=kOutput, calls=%fused_computation.102 | convolution fusion | flops 311132160 | bytes 14698752 | tf_op jit(solution)/shard_map/bqhd,bkhd->bhqk/dot_general | solution.py:75
  87.3 9.1 %copy.136 = f32[4,576,8,128]{3,2,1,0:T(8,128)} copy(f32[4,576,8,128]{3,1,2,0:T(8,128)S(1)} %multiply_bitcast_fusion) | data formatting | bytes 18874368 | tf_op jit(solution)/shard_map/mul | solution.py:137
  96.4 11.1 %reshape.118 = f32[4,9,64,1024]{3,2,1,0:T(8,128)} reshape(f32[4,576,8,128]{3,2,1,0:T(8,128)} %copy.136) | data formatting | bytes 18874368 | tf_op jit(solution)/shard_map/reshape | solution.py:137
  107.5 4.7 %slice_bitcast_fusion.17 = (f32[4,64,1024]{2,1,0:T(8,128)S(1)}, f32[4,64,1024]{2,1,0:T(8,128)S(1)}, f32[4,64,1024]{2,1,0:T(8,128)S(1)}, f32[4,64,1024]{2,1,0:T(8...) fusion(f32[4,9,64,1024]{3,2,1,0:T(8,128)} %reshape.118), kind=kLoop, calls=%fused_computation.46 | loop fusion | bytes 18874368 | tf_op jit(solution)/shard_map/squeeze | solution.py:144
  113.3 1.8 fusion.47
  118.2 2.0 fusion.28
  126.7 92.8 %all-gather = f32[256,320]{1,0:T(8,128)S(1)} all-gather(f32[8,320]{1,0:T(8,128)S(1)} %fusion.37), channel_id=2, replica_groups=mesh['sp'=16,'tp'=2] {'sp','tp'}, dimensions={0}, use_global_device_ids=true | all-gather | bytes 337920 | tf_op jit(solution)/shard_map/all_gather | solution.py:165
  220.1 2.6 %fusion.34 = bf16[256,1024]{1,0:T(8,128)(2,1)} fusion(f32[256,1024]{1,0:T(8,128)} %collective-permute-done.7, f32[256,1024]{1,0:T(8,128)} %collective-permute-done.6, f32[4,64,1024]{2,1,0:T(8,128)S(1)} %copy-done.4), kind=kLoop, calls=%fused_computation.49 | loop fusion | flops 786432 | bytes 3670016 | tf_op jit(solution)/shard_map/convert_element_type | solution.py:169
  222.7 2.6 %fusion.36 = bf16[256,1024]{1,0:T(8,128)(2,1)} fusion(f32[256,1024]{1,0:T(8,128)} %collective-permute-done.5, f32[256,1024]{1,0:T(8,128)} %collective-permute-done.4, f32[4,64,1024]{2,1,0:T(8,128)S(1)} %copy-done.5), kind=kLoop, calls=%fused_computation.52 | loop fusion | flops 786432 | bytes 3670016 | tf_op jit(solution)/shard_map/convert_element_type | solution.py:168
  (104 shorter events, 32.8 us)
Async XLA Ops:
  0.6 14.0 %copy-start = (f32[8,320]{1,0:T(8,128)S(1)}, f32[8,320]{1,0:T(8,128)}, u32[]{:S(2)}) copy-start(f32[8,320]{1,0:T(8,128)} %param.13) | copy-start | bytes 30724
  0.6 29.2 %collective-permute-start.1 = (bf16[256,1024]{1,0:T(8,128)(2,1)}, bf16[256,1024]{1,0:T(8,128)(2,1)}, u32[]{:S(2)}, u32[]{:S(2)}) collective-permute-start(bf16[256,1024]{1,0:T(8,128)(2,1)} %param.8), channel_id=1, source_target_pairs={{0,1},{1,2},{2,3},{3,4},{4,5},{5,6},{6,7},{7,8},{8,9},{9,10},{10,1... | collective-permute-start | bytes 1572872 | tf_op jit(solution)/shard_map/ppermute | solution.py:14
  6.3 17.4 %collective-permute-start = (bf16[256,1024]{1,0:T(8,128)(2,1)}, bf16[256,1024]{1,0:T(8,128)(2,1)}, u32[]{:S(2)}, u32[]{:S(2)}) collective-permute-start(bf16[256,1024]{1,0:T(8,128)(2,1)} %param.8), channel_id=1, source_target_pairs={{0,2},{1,3},{2,4},{3,5},{4,6},{5,7},{6,8},{7,9},{8,10},{9,11},{10,... | collective-permute-start | bytes 1572872 | tf_op jit(solution)/shard_map/ppermute | solution.py:14
  8.4 19.8 %collective-permute-start.3 = (bf16[256,1024]{1,0:T(8,128)(2,1)}, bf16[256,1024]{1,0:T(8,128)(2,1)}, u32[]{:S(2)}, u32[]{:S(2)}) collective-permute-start(bf16[256,1024]{1,0:T(8,128)(2,1)} %param.9), channel_id=1, source_target_pairs={{0,1},{1,2},{2,3},{3,4},{4,5},{5,6},{6,7},{7,8},{8,9},{9,10},{10,1... | collective-permute-start | bytes 1572872 | tf_op jit(solution)/shard_map/ppermute | solution.py:14
  12.6 10.0 %collective-permute-start.2 = (bf16[256,1024]{1,0:T(8,128)(2,1)}, bf16[256,1024]{1,0:T(8,128)(2,1)}, u32[]{:S(2)}, u32[]{:S(2)}) collective-permute-start(bf16[256,1024]{1,0:T(8,128)(2,1)} %param.9), channel_id=1, source_target_pairs={{0,2},{1,3},{2,4},{3,5},{4,6},{5,7},{6,8},{7,9},{8,10},{9,11},{10,... | collective-permute-start | bytes 1572872 | tf_op jit(solution)/shard_map/ppermute | solution.py:14
  22.2 7.2 %copy-start.10 = (bf16[256,1024]{1,0:T(8,128)(2,1)S(1)}, bf16[256,1024]{1,0:T(8,128)(2,1)}, u32[]{:S(2)}) copy-start(bf16[256,1024]{1,0:T(8,128)(2,1)} %param.9) | copy-start | bytes 1572868
  41.0 4.4 %copy-start.8 = (bf16[32,8,8,128]{3,2,1,0:T(8,128)(2,1)S(1)}, bf16[32,8,8,128]{3,2,1,0:T(8,128)(2,1)}, u32[]{:S(2)}) copy-start(bf16[32,8,8,128]{3,2,1,0:T(8,128)(2,1)} %copy.175) | copy-start | bytes 1572868
  43.1 2.3 %copy-start.2 = (f32[4,8,576,64]{2,3,1,0:T(8,128)}, f32[4,8,576,64]{2,3,1,0:T(8,128)S(1)}, u32[]{:S(2)}) copy-start(f32[4,8,576,64]{2,3,1,0:T(8,128)S(1)} %fusion.5) | copy-start | bytes 14155780
  68.2 13.2 %slice-start = ((s8[5242880]{0:T(1024)(128)(4,1)}), s8[4194304]{0:T(1024)(128)(4,1)S(1)}, s32[]{:S(2)}) async-start(s8[5242880]{0:T(1024)(128)(4,1)} %bitcast.211), calls=%async_computation | async-start | bytes 8388608
  68.2 13.2 %slice-start.4 = ((s8[4718592]{0:T(1024)(128)(4,1)}), s8[4194304]{0:T(1024)(128)(4,1)S(1)}, s32[]{:S(2)}) async-start(s8[4718592]{0:T(1024)(128)(4,1)} %bitcast.224), calls=%async_computation.4 | async-start | bytes 8388608
  74.6 6.8 %slice-start.1 = ((s8[5242880]{0:T(1024)(128)(4,1)}), s8[1048576]{0:T(1024)(128)(4,1)S(1)}, s32[]{:S(2)}) async-start(s8[5242880]{0:T(1024)(128)(4,1)} %bitcast.211), calls=%async_computation.1 | async-start | bytes 2097152
  74.6 6.8 %slice-start.5 = ((s8[4718592]{0:T(1024)(128)(4,1)}), s8[524288]{0:T(1024)(128)(4,1)S(1)}, s32[]{:S(2)}) async-start(s8[4718592]{0:T(1024)(128)(4,1)} %bitcast.224), calls=%async_computation.5 | async-start | bytes 1048576
  77.0 4.4 %copy-start.9 = (bf16[32,8,8,128]{3,2,1,0:T(8,128)(2,1)S(1)}, bf16[32,8,8,128]{3,2,1,0:T(8,128)(2,1)}, u32[]{:S(2)}) copy-start(bf16[32,8,8,128]{3,2,1,0:T(8,128)(2,1)} %copy.175) | copy-start | bytes 1572868
  78.8 141.3 %collective-permute-start.7 = (f32[256,1024]{1,0:T(8,128)}, f32[256,1024]{1,0:T(8,128)}, u32[]{:S(2)}, u32[]{:S(2)}) collective-permute-start(f32[256,1024]{1,0:T(8,128)} %bitcast.67), channel_id=1, source_target_pairs={{2,0},{3,1},{4,2},{5,3},{6,4},{7,5},{8,6},{9,7},{10,8},{11,9},{12,... | collective-permute-start | bytes 3145736 | tf_op jit(solution)/shard_map/ppermute | solution.py:14
  80.1 140.1 %collective-permute-start.6 = (f32[256,1024]{1,0:T(8,128)}, f32[256,1024]{1,0:T(8,128)}, u32[]{:S(2)}, u32[]{:S(2)}) collective-permute-start(f32[256,1024]{1,0:T(8,128)} %bitcast.66), channel_id=1, source_target_pairs={{1,0},{2,1},{3,2},{4,3},{5,4},{6,5},{7,6},{8,7},{9,8},{10,9},{11,1... | collective-permute-start | bytes 3145736 | tf_op jit(solution)/shard_map/ppermute | solution.py:14
  107.5 10.7 %slice-start.2 = ((s8[4718592]{0:T(1024)(128)(4,1)}), s8[524288]{0:T(1024)(128)(4,1)S(1)}, s32[]{:S(2)}) async-start(s8[4718592]{0:T(1024)(128)(4,1)} %bitcast.214), calls=%async_computation.2 | async-start | bytes 1048576
  112.2 5.9 %slice-start.3 = ((s8[4718592]{0:T(1024)(128)(4,1)}), s8[4194304]{0:T(1024)(128)(4,1)S(1)}, s32[]{:S(2)}) async-start(s8[4718592]{0:T(1024)(128)(4,1)} %bitcast.214), calls=%async_computation.3 | async-start | bytes 8388608
  113.3 4.9 %copy-start.7 = (bf16[4,8,64,576]{3,2,1,0:T(8,128)(2,1)S(1)}, bf16[4,8,64,576]{3,2,1,0:T(8,128)(2,1)}, u32[]{:S(2)}) copy-start(bf16[4,8,64,576]{3,2,1,0:T(8,128)(2,1)} %copy-done.6) | copy-start | bytes 7077892
  115.0 107.6 %collective-permute-start.5 = (f32[256,1024]{1,0:T(8,128)}, f32[256,1024]{1,0:T(8,128)}, u32[]{:S(2)}, u32[]{:S(2)}) collective-permute-start(f32[256,1024]{1,0:T(8,128)} %bitcast.54), channel_id=1, source_target_pairs={{2,0},{3,1},{4,2},{5,3},{6,4},{7,5},{8,6},{9,7},{10,8},{11,9},{12,... | collective-permute-start | bytes 3145736 | tf_op jit(solution)/shard_map/ppermute | solution.py:14
  116.5 3.8 %copy-start.12 = (f32[8,64,576]{2,1,0:T(8,128)S(1)}, f32[8,64,576]{2,1,0:T(8,128)}, u32[]{:S(2)}) copy-start(f32[8,64,576]{2,1,0:T(8,128)} %get-tuple-element.44) | copy-start | bytes 3538948
  116.5 106.2 %collective-permute-start.4 = (f32[256,1024]{1,0:T(8,128)}, f32[256,1024]{1,0:T(8,128)}, u32[]{:S(2)}, u32[]{:S(2)}) collective-permute-start(f32[256,1024]{1,0:T(8,128)} %bitcast.53), channel_id=1, source_target_pairs={{1,0},{2,1},{3,2},{4,3},{5,4},{6,5},{7,6},{8,7},{9,8},{10,9},{11,1... | collective-permute-start | bytes 3145736 | tf_op jit(solution)/shard_map/ppermute | solution.py:14
  123.6 96.5 %copy-start.4 = (f32[4,64,1024]{2,1,0:T(8,128)S(1)}, f32[4,64,1024]{2,1,0:T(8,128)}, u32[]{:S(2)}) copy-start(f32[4,64,1024]{2,1,0:T(8,128)} %get-tuple-element.22) | copy-start | bytes 3145732
  123.7 99.1 %copy-start.5 = (f32[4,64,1024]{2,1,0:T(8,128)S(1)}, f32[4,64,1024]{2,1,0:T(8,128)}, u32[]{:S(2)}) copy-start(f32[4,64,1024]{2,1,0:T(8,128)} %get-tuple-element.25) | copy-start | bytes 3145732
  125.3 100.0 %copy-start.1 = (f32[8,320]{1,0:T(8,128)S(1)}, f32[8,320]{1,0:T(8,128)}, u32[]{:S(2)}) copy-start(f32[8,320]{1,0:T(8,128)} %param.13) | copy-start | bytes 30724
  (3 other events, 5.2 us)
